TPU v7x, 256 devices: a 4x2x16 block of a 4x16x16 slice. The times are simulated.
256 devices in a mesh: grp: 2 (over y), kv: 16 (over z), tp: 8 (over x, core).
Axes of the slice: x: 4, y: 2, z: 16, core: 2. Of those that a mesh axis runs over, the one named last changes fastest.
The devices are a block of a 4x16x16 slice.
Arguments:
- tokens: bfloat16 [512, 2048], P('grp', 'kv'), parts along dimension 0, may hold values from -64 to 64
- lengths: int32 [512], P(('grp', 'kv')), parts along dimension 0, may hold values from 1 to 4096, 131072 in all
- state: float32 [512, 8, 128, 256], P(('grp', 'kv'), 'tp'), parts along dimension 0, may hold values from -6 to 6
- key_block: bfloat16 [512, 8, 64, 128], P(('grp', 'kv'), 'tp'), parts along dimension 0, may hold values from -6 to 6
- value_block: bfloat16 [512, 8, 64, 256], P(('grp', 'kv'), 'tp'), parts along dimension 0, may hold values from -6 to 6
- cum_decay: float32 [512, 8, 64, 128], P(('grp', 'kv'), 'tp'), parts along dimension 0, as said below
- step_decay: float32 [512, 1024], P(('grp', 'kv'), 'tp'), parts along dimension 0
- g_mix: bfloat16 [2048], P('kv'), may hold values from 0.099609375 to 1.8984375
- w_query: bfloat16 [2048, 1024], P('kv', 'tp'), may hold values from -0.125 to 0.125
- w_key: bfloat16 [2048, 1024], P('kv', 'tp'), may hold values from -0.125 to 0.125
- w_value: bfloat16 [2048, 2048], P('kv', 'tp'), may hold values from -0.125 to 0.125
- w_outgate: bfloat16 [2048, 2048], P('kv', 'tp'), may hold values from -0.125 to 0.125
- w_decay: bfloat16 [2048, 1024], P('kv', 'tp'), may hold values from -0.5 to 0.5
- g_heads: bfloat16 [2048], P('tp'), may hold values from 0.099609375 to 1.8984375
- w_out: bfloat16 [2048, 2048], P('tp', 'kv'), may hold values from -0.125 to 0.125
- g_ffn: bfloat16 [2048], P('kv'), may hold values from 0.099609375 to 1.8984375
- w_gate: bfloat16 [2048, 5632], P('kv', 'tp'), may hold values from -0.125 to 0.125
- w_up: bfloat16 [2048, 5632], P('kv', 'tp'), may hold values from -0.125 to 0.125
- w_down: bfloat16 [5632, 2048], P('tp', 'kv'), may hold values from -0.078125 to 0.078125
Outputs:
- updated: bfloat16 [512, 2048], P('grp', 'kv'), parts along dimension 0
There are 2 independent parts, one for each index of `grp`. A program takes and returns all parts, laid end to end along the dimension named above; an argument that names none is the same for every part. Nothing has to cross between parts.
Inputs may be any that keep to these rules, and one draw needn't show every extreme that they name: `cum_decay`: along the block's positions the entries never rise.
All inputs are finite; a program needn't handle non-finite values. No bound on the sum of `lengths` on one device may be relied on, other than what follows from the above.
Results may differ from a plain program's by a relative error of at most 0.019.
Values may be sent and summed in bfloat16 or wider, within the bound.
A program may use at most 64 MiB of HBM per device.

v0:
```python
import jax
import jax.numpy as jnp
from jax import lax
from jax.sharding import PartitionSpec as P

D = 2048
DK = 128
DV = 256


epsilon = 1e-06
temper = 16.0


def sent_to_all(shard, axis):
    copies = jnp.broadcast_to(shard, (lax.axis_size(axis), *shard.shape))
    return lax.all_to_all(copies, axis, split_axis=0, concat_axis=0, tiled=True)


def over_copies(shard, axis):
    return sent_to_all(shard, axis).sum(axis=0)


def in_blocks(shard, dim, peers):
    lengths = shard.shape
    pieces = shard.reshape(*lengths[:dim], peers, lengths[dim] // peers, *lengths[dim + 1 :])
    return jnp.moveaxis(pieces, dim, 0)


def summed_on_arrival(shard, axis, dim):
    pieces = in_blocks(shard, dim, lax.axis_size(axis))
    arrived = lax.all_to_all(pieces, axis, split_axis=0, concat_axis=0, tiled=True)
    return arrived.astype(jnp.float32).sum(axis=0)


def joined_along(pieces, dim):
    pieces = jnp.moveaxis(pieces, 0, dim)
    lengths = pieces.shape
    return pieces.reshape(*lengths[:dim], lengths[dim] * lengths[dim + 1], *lengths[dim + 2 :])


def gathered_copies(shard, axis, dim):
    return joined_along(sent_to_all(shard, axis), dim)


def over_copies_2(shard, axis):
    everything = sent_to_all(shard, axis)
    return jnp.sum(everything.astype(jnp.float32), axis=0)


def sent_together(arrays, axis, dim, along):
    columns = [a.reshape(*a.shape[:along], -1) for a in arrays]
    both = jnp.concatenate(columns, axis=along)
    filled, at, gathered = (summed_on_arrival(both, axis, dim), 0, [])
    for a, column in zip(arrays, columns):
        section = filled[..., at : at + column.shape[along]]
        gathered.append(section.reshape(*section.shape[:along], *a.shape[along:]))
        at += column.shape[along]
    return tuple(gathered)


def body(
    tokens,
    lengths,
    state,
    key_block,
    value_block,
    cum_decay,
    step_decay,
    g_mix,
    w_query,
    w_key,
    w_value,
    w_outgate,
    w_decay,
    g_heads,
    w_out,
    g_ffn,
    w_gate,
    w_up,
    w_down,
):
    highest = lax.Precision.HIGHEST
    seqs = state.shape[0]
    heads = state.shape[1]
    block_len = key_block.shape[2]
    key_width = heads * DK
    value_width = heads * DV
    inputs = tokens.astype(jnp.float32)
    square = jnp.sum(inputs * inputs, axis=1)
    scaled = (inputs * g_mix.astype(jnp.float32)).astype(jnp.bfloat16)
    matrices = (w_query, w_key, w_value, w_outgate, w_decay)
    row_total = over_copies(square, "kv")
    own_total = lax.dynamic_slice_in_dim(row_total, lax.axis_index("kv") * seqs, seqs, 0)
    projected = summed_on_arrival(
        jnp.concatenate(
            [jnp.dot(scaled, matrix, preferred_element_type=jnp.float32) for matrix in matrices],
            axis=1,
        ).astype(jnp.bfloat16),
        "kv",
        0,
    )
    projected = projected * lax.rsqrt(own_total / D + epsilon)[:, None]
    query = (projected[:, :key_width] * DK ** (-0.5)).reshape(seqs, heads, DK)
    keys_new = projected[:, key_width : 2 * key_width].reshape(seqs, heads, DK)
    values_new = projected[:, 2 * key_width : 2 * key_width + value_width].reshape(seqs, heads, DV)
    out_gate = projected[:, 2 * key_width + value_width : 2 * key_width + 2 * value_width]
    decay_pre = projected[:, 2 * key_width + 2 * value_width :]
    log_step = (jax.nn.log_sigmoid(decay_pre) / temper + step_decay).reshape(seqs, heads, DK)
    live_count = lengths % block_len
    token_ordinal = lax.broadcasted_iota(jnp.int32, (1, 1, block_len, 1), 2)
    picked = jnp.where(
        token_ordinal == live_count[:, None, None, None] - 1, cum_decay, jnp.float32(0.0)
    )
    token_decay = jnp.sum(picked, axis=2) + log_step
    carried = jnp.einsum("shk,shkv->shv", query * jnp.exp(token_decay), state, precision=highest)
    scores = jnp.sum(
        query[:, :, None, :]
        * key_block.astype(jnp.float32)
        * jnp.exp(token_decay[:, :, None, :] - cum_decay),
        axis=3,
    )
    scores = jnp.where(token_ordinal[..., 0] < live_count[:, None, None], scores, jnp.float32(0.0))
    in_block = jnp.einsum(
        "shj,shjv->shv", scores, value_block.astype(jnp.float32), precision=highest
    )
    own_term = jnp.sum(query * keys_new, axis=2)[:, :, None] * values_new
    head_out = carried + in_block + own_term
    normed = head_out * lax.rsqrt(jnp.mean(head_out * head_out, axis=2, keepdims=True) + epsilon)
    normed = normed * g_heads.astype(jnp.float32).reshape(heads, DV)
    mixed = (normed.reshape(seqs, value_width) * jax.nn.silu(out_gate)).astype(jnp.bfloat16)
    attn_part = jnp.dot(
        gathered_copies(mixed, "kv", 0), w_out, preferred_element_type=jnp.float32
    ).astype(jnp.bfloat16)
    attention = over_copies_2(attn_part, "tp").astype(jnp.float32)
    residual = (inputs + attention).astype(jnp.bfloat16)
    middle = residual.astype(jnp.float32)
    square_mid = jnp.sum(middle * middle, axis=1)
    normed_mid = (middle * g_ffn.astype(jnp.float32)).astype(jnp.bfloat16)
    gate_part = jnp.dot(normed_mid, w_gate, preferred_element_type=jnp.float32)
    up_part = jnp.dot(normed_mid, w_up, preferred_element_type=jnp.float32)
    gate_total, up_total, mid_total = sent_together(
        (
            gate_part.astype(jnp.bfloat16),
            up_part.astype(jnp.bfloat16),
            square_mid.astype(jnp.bfloat16),
        ),
        "kv",
        0,
        1,
    )
    mid_inverse = lax.rsqrt(mid_total / D + epsilon)[:, None]
    hidden = (jax.nn.silu(gate_total * mid_inverse) * (up_total * mid_inverse)).astype(jnp.bfloat16)
    down_part = jnp.dot(
        gathered_copies(hidden, "kv", 0), w_down, preferred_element_type=jnp.float32
    ).astype(jnp.bfloat16)
    down_total = over_copies_2(down_part, "tp").astype(jnp.float32)
    return (middle + down_total).astype(jnp.bfloat16)


def solution(mesh):
    return jax.shard_map(
        body,
        mesh=mesh,
        in_specs=(
            P("grp", "kv"),
            P(("grp", "kv")),
            P(("grp", "kv"), "tp", None, None),
            P(("grp", "kv"), "tp", None, None),
            P(("grp", "kv"), "tp", None, None),
            P(("grp", "kv"), "tp", None, None),
            P(("grp", "kv"), "tp"),
            P("kv"),
            P("kv", "tp"),
            P("kv", "tp"),
            P("kv", "tp"),
            P("kv", "tp"),
            P("kv", "tp"),
            P("tp"),
            P("tp", "kv"),
            P("kv"),
            P("kv", "tp"),
            P("kv", "tp"),
            P("tp", "kv"),
        ),
        out_specs=P("grp", "kv"),
        check_vma=False,
    )
```

profile of v0, /device:TPU:33, one launch (start us, length us, event | category | flops | bytes accessed | tf_op | source)
XLA Modules:
  0.0 203.8 jit_solution(13432914267603530753)
XLA Ops:
  0.0 1.1 fusion.5
  1.1 0.6 broadcast_in_dim.40
  1.8 24.5 %all-to-all-start.1 = ((f32[16,1,256]{2,1,0:T(1,128)}), f32[16,1,256]{2,1,0:T(1,128)S(1)}, u32[]{:S(2)}, u32[]{:S(2)}) async-start(f32[16,1,256]{2,1,0:T(1,128)} %broadcast_in_dim.40), calls=%async_computation.1 | async-start | bytes 32768 | tf_op jit(solution)/shard_map/all_to_all | solution.py:17
  26.3 0.7 convert_element_type.78
  26.9 1.0 convolution_convert_fusion.6
  27.9 1.0 convolution_convert_fusion.5
  28.9 1.0 convolution_convert_fusion.7
  29.9 1.0 convolution_convert_fusion.3
  31.0 1.0 convolution_convert_fusion.2
  32.0 0.6 constant_dynamic-update-slice_fusion.4
  32.7 0.6 constant_dynamic-update-slice_fusion.3
  33.3 0.7 constant_dynamic-update-slice_fusion.2
  34.0 0.7 constant_dynamic-update-slice_fusion.1
  34.6 0.6 constant_dynamic-update-slice_fusion
  35.3 2.2 %all-to-all-done.1 = f32[16,1,256]{2,1,0:T(1,128)S(1)} async-done(((f32[16,1,256]{2,1,0:T(1,128)}), f32[16,1,256]{2,1,0:T(1,128)S(1)}, u32[]{:S(2)}, u32[]{:S(2)}) %all-to-all-start.1) | async-done | bytes 16416 | tf_op jit(solution)/shard_map/all_to_all | solution.py:17
  37.5 9.3 %all-to-all-start = ((bf16[16,16,896]{2,1,0:T(8,128)(2,1)}), bf16[16,16,896]{2,1,0:T(8,128)(2,1)S(1)}, u32[]{:S(2)}, u32[]{:S(2)}) async-start(bf16[16,16,896]{2,1,0:T(8,128)(2,1)} %constant_dynamic-update-slice_fusion), calls=%async_computation | async-start | bytes 917504 | tf_op jit(solution)/shard_map/all_to_all | solution.py:32
  46.8 0.1 iota_compare_fusion.1
  46.9 0.2 select_reduce_fusion
  47.1 0.1 add_rsqrt_fusion.1
  47.2 20.3 %all-to-all-done = bf16[16,16,896]{2,1,0:T(8,128)(2,1)S(1)} async-done(((bf16[16,16,896]{2,1,0:T(8,128)(2,1)}), bf16[16,16,896]{2,1,0:T(8,128)(2,1)S(1)}, u32[]{:S(2)}, u32[]{:S(2)}) %all-to-all-start) | async-done | bytes 458784 | tf_op jit(solution)/shard_map/all_to_all | solution.py:32
  67.6 0.1 broadcast_multiply_fusion
  67.7 0.1 slice_multiply_fusion.5
  67.8 0.2 multiply_reduce_fusion
  68.0 0.1 fusion.28
  68.1 1.4 fusion.2
  69.5 1.1 fusion
  70.6 0.2 multiply_reduce_fusion.1
  70.8 0.1 multiply_convert_fusion
  70.9 23.2 %all_to_all.36 = bf16[16,16,256]{2,1,0:T(8,128)(2,1)S(1)} all-to-all(bf16[16,16,256]{2,1,0:T(8,128)(2,1)S(1)} %broadcast_in_dim.44), channel_id=1, replica_groups=mesh['grp'=2,'kv'=16,'tp'=8] {'kv'}, dimensions={0} | all-to-all | bytes 262144 | tf_op jit(solution)/shard_map/all_to_all | solution.py:17
  94.1 0.2 convolution_convert_fusion.8
  94.2 0.9 broadcast_in_dim.45
  95.1 8.3 %all-to-all-start.3 = ((bf16[8,256,128]{2,1,0:T(8,128)(2,1)}), bf16[8,256,128]{2,1,0:T(8,128)(2,1)S(1)}, u32[]{:S(2)}, u32[]{:S(2)}) async-start(bf16[8,256,128]{2,1,0:T(8,128)(2,1)} %broadcast_in_dim.45), calls=%async_computation.3 | async-start | bytes 1048576 | tf_op jit(solution)/shard_map/all_to_all | solution.py:17
  103.4 9.3 %all-to-all-done.3 = bf16[8,256,128]{2,1,0:T(8,128)(2,1)S(1)} async-done(((bf16[8,256,128]{2,1,0:T(8,128)(2,1)}), bf16[8,256,128]{2,1,0:T(8,128)(2,1)S(1)}, u32[]{:S(2)}, u32[]{:S(2)}) %all-to-all-start.3) | async-done | bytes 524320 | tf_op jit(solution)/shard_map/all_to_all | solution.py:17
  112.8 0.1 fusion.8
  112.9 0.2 convert_element_type.99
  113.2 0.3 convolution_convert_fusion
  113.4 0.2 copy.39
  113.6 0.3 convolution_convert_fusion.1
  113.9 0.9 copy.38
  114.8 1.3 concatenate.31
  116.1 38.6 %all_to_all.37 = bf16[16,16,1409]{2,1,0:T(8,128)(2,1)S(1)} all-to-all(bf16[16,16,1409]{2,1,0:T(8,128)(2,1)S(1)} %concatenate.31), channel_id=1, replica_groups=mesh['grp'=2,'kv'=16,'tp'=8] {'kv'}, dimensions={0} | all-to-all | bytes 1442816 | tf_op jit(solution)/shard_map/all_to_all | solution.py:32
  154.7 0.1 convert_reduce_fusion
  154.8 0.1 fusion.26
  155.0 0.1 fusion.13
  155.1 29.2 %all_to_all.38 = bf16[16,16,704]{2,1,0:T(8,128)(2,1)S(1)} all-to-all(bf16[16,16,704]{2,1,0:T(8,128)(2,1)S(1)} %broadcast_in_dim.46), channel_id=1, replica_groups=mesh['grp'=2,'kv'=16,'tp'=8] {'kv'}, dimensions={0} | all-to-all | bytes 720896 | tf_op jit(solution)/shard_map/all_to_all | solution.py:17
  184.3 0.2 convolution_convert_fusion.4
  184.7 18.4 %all_to_all.39 = bf16[8,256,128]{2,1,0:T(8,128)(2,1)S(1)} all-to-all(bf16[8,256,128]{2,1,0:T(8,128)(2,1)S(1)} %broadcast_in_dim.47), channel_id=1, replica_groups=mesh['grp'=2,'kv'=16,'tp'=8] {'tp'}, dimensions={0} | all-to-all | bytes 1048576 | tf_op jit(solution)/shard_map/all_to_all | solution.py:17
  203.1 0.7 fusion.9
  (35 shorter events, 0.4 us)
Async XLA Ops:
  0.0 69.4 %copy-start = (f32[16,1,128,256]{3,2,1,0:T(8,128)S(1)}, f32[16,1,128,256]{3,2,1,0:T(8,128)}, u32[]{:S(2)}) copy-start(f32[16,1,128,256]{3,2,1,0:T(8,128)} %param.21) | copy-start | bytes 6291460
  0.0 46.8 %copy-start.9 = (bf16[256]{0:T(256)(128)(2,1)S(1)}, bf16[256]{0:T(256)(128)(2,1)}, u32[]{:S(2)}) copy-start(bf16[256]{0:T(256)(128)(2,1)} %param.32) | copy-start | bytes 1540
  0.0 46.8 %copy-start.10 = (s32[16]{0:T(128)S(1)}, s32[16]{0:T(128)}, u32[]{:S(2)}) copy-start(s32[16]{0:T(128)} %param.20) | copy-start | bytes 196
  0.0 46.9 %copy-start.2 = (f32[16,1,64,128]{3,2,1,0:T(8,128)S(1)}, f32[16,1,64,128]{3,2,1,0:T(8,128)}, u32[]{:S(2)}) copy-start(f32[16,1,64,128]{3,2,1,0:T(8,128)} %param.24) | copy-start | bytes 1572868
  0.0 67.6 %copy-start.8 = (f32[16,128]{1,0:T(8,128)S(1)}, f32[16,128]{1,0:T(8,128)}, u32[]{:S(2)}) copy-start(f32[16,128]{1,0:T(8,128)} %param.25) | copy-start | bytes 24580
  1.1 66.6 %copy-start.3 = (bf16[16,1,64,128]{3,2,1,0:T(8,128)(2,1)S(1)}, bf16[16,1,64,128]{3,2,1,0:T(8,128)(2,1)}, u32[]{:S(2)}) copy-start(bf16[16,1,64,128]{3,2,1,0:T(8,128)(2,1)} %param.22) | copy-start | bytes 786436
  1.8 35.7 %all-to-all-start.1 = ((f32[16,1,256]{2,1,0:T(1,128)}), f32[16,1,256]{2,1,0:T(1,128)S(1)}, u32[]{:S(2)}, u32[]{:S(2)}) async-start(f32[16,1,256]{2,1,0:T(1,128)} %broadcast_in_dim.40), calls=%async_computation.1 | async-start | bytes 32768 | tf_op jit(solution)/shard_map/all_to_all | solution.py:17
  37.5 30.0 %all-to-all-start = ((bf16[16,16,896]{2,1,0:T(8,128)(2,1)}), bf16[16,16,896]{2,1,0:T(8,128)(2,1)S(1)}, u32[]{:S(2)}, u32[]{:S(2)}) async-start(bf16[16,16,896]{2,1,0:T(8,128)(2,1)} %constant_dynamic-update-slice_fusion), calls=%async_computation | async-start | bytes 917504 | tf_op jit(solution)/shard_map/all_to_all | solution.py:32
  67.6 26.5 %copy-start.7 = (bf16[256,128]{1,0:T(8,128)(2,1)S(1)}, bf16[256,128]{1,0:T(8,128)(2,1)}, u32[]{:S(2)}) copy-start(bf16[256,128]{1,0:T(8,128)(2,1)} %param.33) | copy-start | bytes 196612
  69.4 33.9 %copy-start.11 = (bf16[128]{0:T(256)(128)(2,1)S(1)}, bf16[128]{0:T(256)(128)(2,1)}, u32[]{:S(2)}) copy-start(bf16[128]{0:T(256)(128)(2,1)} %param.34) | copy-start | bytes 772
  69.4 43.3 %copy-start.1 = (bf16[256,128]{1,0:T(8,128)(2,1)S(1)}, bf16[256,128]{1,0:T(8,128)(2,1)}, u32[]{:S(2)}) copy-start(bf16[256,128]{1,0:T(8,128)(2,1)} %param.19) | copy-start | bytes 196612
  70.6 42.6 %copy-start.4 = (bf16[128,704]{0,1:T(8,128)(2,1)S(1)}, bf16[128,704]{0,1:T(8,128)(2,1)}, u32[]{:S(2)}) copy-start(bf16[128,704]{0,1:T(8,128)(2,1)} %param.36) | copy-start | bytes 540676
  94.1 19.5 %copy-start.5 = (bf16[128,704]{0,1:T(8,128)(2,1)S(1)}, bf16[128,704]{0,1:T(8,128)(2,1)}, u32[]{:S(2)}) copy-start(bf16[128,704]{0,1:T(8,128)(2,1)} %param.35) | copy-start | bytes 540676
  95.1 17.6 %all-to-all-start.3 = ((bf16[8,256,128]{2,1,0:T(8,128)(2,1)}), bf16[8,256,128]{2,1,0:T(8,128)(2,1)S(1)}, u32[]{:S(2)}, u32[]{:S(2)}) async-start(bf16[8,256,128]{2,1,0:T(8,128)(2,1)} %broadcast_in_dim.45), calls=%async_computation.3 | async-start | bytes 1048576 | tf_op jit(solution)/shard_map/all_to_all | solution.py:17
  116.1 68.2 %copy-start.6 = (bf16[704,128]{1,0:T(8,128)(2,1)S(1)}, bf16[704,128]{1,0:T(8,128)(2,1)}, u32[]{:S(2)}) copy-start(bf16[704,128]{1,0:T(8,128)(2,1)} %param.37) | copy-start | bytes 540676
where the time goes:
time: 205 us; the launch traced here: 204 us
  blocking collectives  109 us (53%)
  starting transfers between devices  42 us (20%)
  waiting for transfers between devices  31.8 us (16%)
  matrix products  8.44 us (4%)
  local copies, waits for them, and re-layouts  7.53 us (4%)
  other arithmetic  4.23 us (2%)
    all_to_all x3, blocking collectives, sent_to_all(): return lax.all_to_all(copies, axis, split_axis=0, concat_axis=0, tiled=True)  70.8 us
    all_to_all x1, blocking collectives, summed_on_arrival(): lax.all_to_all(pieces, axis, split_axis=0, concat_axis=0, tiled=True)  38.6 us
    all_to_all x2, starting transfers between devices, sent_to_all(): return lax.all_to_all(copies, axis, split_axis=0, concat_axis=0, tiled=True)  32.8 us
    all_to_all x1, waiting for transfers between devices, summed_on_arrival(): lax.all_to_all(pieces, axis, split_axis=0, concat_axis=0, tiled=True)  20.3 us
    all_to_all x2, waiting for transfers between devices, sent_to_all(): return lax.all_to_all(copies, axis, split_axis=0, concat_axis=0, tiled=True)  11.5 us
    all_to_all x1, starting transfers between devices, summed_on_arrival(): lax.all_to_all(pieces, axis, split_axis=0, concat_axis=0, tiled=True)  9.27 us
    dot_general x5, matrix products, body(): jnp.dot(scaled, matrix, preferred_element_type=jnp.float32)  5.05 us
  transfers between devices with their start and end apart: 3, of which 3 were waited for; matrix products, arithmetic and copies ran while one was open for 5% of the time, Pallas kernels for 0%

commit v1 on v0

v1 whole, which is shorter than its diff:
```python
import functools

import jax
import jax.numpy as jnp
from jax import lax
from jax.experimental import pallas as pl
from jax.experimental.pallas import tpu as pltpu
from jax.sharding import PartitionSpec as P

D = 2048
DK = 128
DV = 256

epsilon = 1e-06
temper = 16.0

MESH = pl.DeviceIdType.MESH
LANES = 128
HUBS_PROJ = (3, 6)
HUBS_MIXED = (3, 6)
HUBS_FFN = (3, 6)
HUBS_HIDDEN = (3, 6)
f32 = jnp.float32
bf16 = jnp.bfloat16


class RingTree:
    def __init__(self, n, hubs):
        self.n = n
        self.far = (n // 2, n - 1 - n // 2)
        self.hubs = [[0] + [h for h in hubs if h < far] for far in self.far]

    def index(self, side, delta):
        return delta - 1 + side * self.far[0]

    def parent(self, side, delta):
        return max(h for h in self.hubs[side] if h < delta)

    def children(self, side, hub):
        return [d for d in range(1, self.far[side] + 1) if self.parent(side, d) == hub]

    def leaves(self, side, hub):
        return [d for d in self.children(side, hub) if d not in self.hubs[side]]

    def reach(self):
        return max(d - self.parent(s, d) for s in (0, 1) for d in range(1, self.far[s] + 1))

    def levels(self):
        return max(len(h) for h in self.hubs)


def ring_reduce_scatter(tree, me, part, slots, stage, send_sem, recv_sem):
    n = tree.n

    def node(offset):
        return lax.rem(me + (offset + n), n)

    def copy(side, delta, src):
        sign = 1 - 2 * side
        k = tree.index(side, delta)
        hop = delta - tree.parent(side, delta)
        return pltpu.make_async_remote_copy(
            src_ref=src,
            dst_ref=slots.at[k],
            send_sem=send_sem.at[k],
            recv_sem=recv_sem.at[k],
            device_id={"kv": node(-sign * hop)},
            device_id_type=MESH,
        )

    def owner(side, delta):
        return node(-(1 - 2 * side) * delta)

    started = []

    def send_leaves(level):
        todo = [
            [(s, d) for d in tree.leaves(s, tree.hubs[s][level])] if level < len(tree.hubs[s]) else []
            for s in (0, 1)
        ]
        for i in range(max(len(t) for t in todo)):
            for t in todo:
                if i < len(t):
                    side, delta = t[i]
                    c = copy(side, delta, part.at[owner(side, delta)])
                    c.start()
                    started.append(c)

    def combined(side, hub, own):
        total = own
        for delta in tree.children(side, hub):
            k = tree.index(side, delta)
            copy(side, delta, slots.at[k]).wait_recv()
            total = total + slots[k].astype(f32)
        return total

    top = tree.levels() - 1
    send_leaves(top)
    for level in range(top, 0, -1):
        send_leaves(level - 1)
        for side in (0, 1):
            if level < len(tree.hubs[side]):
                hub = tree.hubs[side][level]
                k = tree.index(side, hub)
                total = combined(side, hub, part[owner(side, hub)].astype(f32))
                spot = 2 * (level - 1) + side
                stage[spot] = total.astype(stage.dtype)
                c = copy(side, hub, stage.at[spot])
                c.start()
                started.append(c)
    total = part[me].astype(f32)
    for side in (0, 1):
        total = combined(side, 0, total)
    return total, started


def ring_all_gather(tree, me, whole, send_sem, recv_sem):
    n = tree.n

    def node(offset):
        return lax.rem(me + (offset + n), n)

    def copy(side, delta):
        sign = 1 - 2 * side
        k = tree.index(side, delta)
        hub = tree.parent(side, delta)
        block = whole.at[node(-sign * hub)]
        return pltpu.make_async_remote_copy(
            src_ref=block,
            dst_ref=block,
            send_sem=send_sem.at[k],
            recv_sem=recv_sem.at[k],
            device_id={"kv": node(sign * (delta - hub))},
            device_id_type=MESH,
        )

    def arrived(side, delta):
        sign = 1 - 2 * side
        k = tree.index(side, delta)
        block = whole.at[node(-sign * delta)]
        pltpu.make_async_remote_copy(
            src_ref=block,
            dst_ref=block,
            send_sem=send_sem.at[k],
            recv_sem=recv_sem.at[k],
            device_id={"kv": node(sign)},
            device_id_type=MESH,
        ).wait_recv()

    started = []
    waited = set()
    for level in range(tree.levels()):
        for side in (0, 1):
            if level < len(tree.hubs[side]):
                hub = tree.hubs[side][level]
                if hub:
                    arrived(side, hub)
                    waited.add((side, hub))
                for delta in reversed(tree.children(side, hub)):
                    c = copy(side, delta)
                    c.start()
                    started.append(c)
    for side in (0, 1):
        for delta in range(1, tree.far[side] + 1):
            if (side, delta) not in waited:
                arrived(side, delta)
    return started


def tp_exchange(n, me, block_for, slot_of, send_sem, recv_sem):
    copies = []
    for j in range(1, n):
        peer = lax.rem(me + j, n)
        copies.append(
            pltpu.make_async_remote_copy(
                src_ref=block_for(peer),
                dst_ref=slot_of(me, j),
                send_sem=send_sem.at[j],
                recv_sem=recv_sem.at[j],
                device_id={"tp": peer},
                device_id_type=MESH,
            )
        )
    for c in copies:
        c.start()
    return copies


def tp_arrived(n, me, slot_of, send_sem, recv_sem):
    for j in range(1, n):
        source = lax.rem(me + (n - j), n)
        slot = slot_of(source, j)
        pltpu.make_async_remote_copy(
            src_ref=slot,
            dst_ref=slot,
            send_sem=send_sem.at[j],
            recv_sem=recv_sem.at[j],
            device_id={"tp": source},
            device_id_type=MESH,
        ).wait_recv()


def tp_all_reduce(n, me, part, slots, whole, finish, send_sem, recv_sem):
    started = tp_exchange(n, me, lambda peer: part.at[peer], lambda source, j: slots.at[j], send_sem.at[0], recv_sem.at[0])
    tp_arrived(n, me, lambda source, j: slots.at[j], send_sem.at[0], recv_sem.at[0])
    total = part[me].astype(f32)
    for j in range(1, n):
        total = total + slots[j].astype(f32)
    whole[me] = finish(total).astype(whole.dtype)
    started += tp_exchange(n, me, lambda peer: whole.at[me], lambda source, j: whole.at[source], send_sem.at[1], recv_sem.at[1])
    tp_arrived(n, me, lambda source, j: whole.at[source], send_sem.at[1], recv_sem.at[1])
    return started


def silu(v):
    return v / (1.0 + jnp.exp(-v))


def kernel(n_kv, n_tp, trees, names, *refs):
    count = len(names)
    hbm = dict(zip(names, refs[:count]))
    lengths = refs[count]
    out = refs[count + 1]
    vm = dict(zip(names, refs[count + 2 : 2 * count + 2]))
    (
        load_sem,
        part_a,
        slots_a,
        stage_a,
        mixed_all,
        part_c,
        slots_c,
        res_all,
        part_d,
        slots_d,
        stage_d,
        hidden_all,
        part_f,
        slots_f,
        out_all,
        send_a,
        recv_a,
        send_b,
        recv_b,
        send_c,
        recv_c,
        send_d,
        recv_d,
        send_e,
        recv_e,
        send_f,
        recv_f,
    ) = refs[2 * count + 2 :]
    kv = lax.axis_index("kv")
    tp = lax.axis_index("tp")
    tree_a, tree_b, tree_d, tree_e = trees

    reach = max(t.reach() for t in trees)
    barrier = pltpu.get_barrier_semaphore()
    peers = 0
    for o in range(1, reach + 1):
        for offset in (o, n_kv - o):
            pl.semaphore_signal(
                barrier, inc=1, device_id={"kv": lax.rem(kv + offset, n_kv)}, device_id_type=MESH
            )
            peers += 1
    for j in range(1, n_tp):
        pl.semaphore_signal(barrier, inc=1, device_id={"tp": lax.rem(tp + j, n_tp)}, device_id_type=MESH)
        peers += 1

    loads = {}
    for i, name in enumerate(names):
        loads[name] = pltpu.make_async_copy(hbm[name], vm[name], load_sem.at[i])
        loads[name].start()

    for name in ("tokens", "g_mix", "w_query", "w_key", "w_value", "w_outgate", "w_decay"):
        loads[name].wait()
    seqs = part_a.shape[1]
    inputs = vm["tokens"][...].astype(f32)
    rows = inputs.shape[0]
    scaled = (inputs * vm["g_mix"][...].astype(f32)).astype(bf16)
    at = 0
    for name in ("w_query", "w_key", "w_value", "w_outgate", "w_decay"):
        weight = vm[name][...]
        width = weight.shape[1]
        product = jnp.dot(scaled, weight, preferred_element_type=f32)
        part_a[:, :, at : at + width] = product.astype(bf16).reshape(n_kv, seqs, width)
        at += width
    square = jnp.broadcast_to(jnp.sum(inputs * inputs, axis=1, keepdims=True), (rows, LANES))
    part_a[:, :, at : at + LANES] = square.astype(bf16).reshape(n_kv, seqs, LANES)

    pl.semaphore_wait(barrier, peers)
    projected, started = ring_reduce_scatter(tree_a, kv, part_a, slots_a, stage_a, send_a, recv_a)

    for name in names:
        if name not in ("tokens", "g_mix", "w_query", "w_key", "w_value", "w_outgate", "w_decay"):
            loads[name].wait()

    inverse = lax.rsqrt(projected[:, at : at + 1] / D + epsilon)
    projected = projected * inverse
    query = projected[:, :DK] * DK ** (-0.5)
    keys_new = projected[:, DK : 2 * DK]
    values_new = projected[:, 2 * DK : 2 * DK + DV]
    out_gate = projected[:, 2 * DK + DV : 2 * DK + 2 * DV]
    decay_pre = projected[:, 2 * DK + 2 * DV : 3 * DK + 2 * DV]
    log_sig = jnp.minimum(decay_pre, 0.0) - jnp.log1p(jnp.exp(-jnp.abs(decay_pre)))
    log_step = log_sig / temper + vm["step_decay"][...]

    block_len = vm["key_block"].shape[2]
    ordinal = lax.broadcasted_iota(jnp.int32, (block_len, DK), 0)
    ordinal_column = lax.broadcasted_iota(jnp.int32, (block_len, 1), 0)
    live = [lax.rem(lengths[s], block_len) for s in range(seqs)]
    picked = [
        jnp.sum(
            jnp.where(ordinal == live[s] - 1, vm["cum_decay"][s, 0], 0.0), axis=0, keepdims=True
        )
        for s in range(seqs)
    ]
    token_decay = jnp.concatenate(picked, axis=0) + log_step
    weighted = jnp.transpose(query * jnp.exp(token_decay))
    heads_out = []
    for s in range(seqs):
        carried = jnp.sum(weighted[:, s : s + 1] * vm["state"][s, 0], axis=0, keepdims=True)
        scores = jnp.sum(
            query[s : s + 1]
            * vm["key_block"][s, 0].astype(f32)
            * jnp.exp(token_decay[s : s + 1] - vm["cum_decay"][s, 0]),
            axis=1,
            keepdims=True,
        )
        scores = jnp.where(ordinal_column < live[s], scores, 0.0)
        in_block = jnp.sum(scores * vm["value_block"][s, 0].astype(f32), axis=0, keepdims=True)
        heads_out.append(carried + in_block)
    head_out = jnp.concatenate(heads_out, axis=0)
    head_out = head_out + jnp.sum(query * keys_new, axis=1, keepdims=True) * values_new
    normed = head_out * lax.rsqrt(jnp.mean(head_out * head_out, axis=1, keepdims=True) + epsilon)
    normed = normed * vm["g_heads"][...].astype(f32)
    mixed_all[kv] = (normed * silu(out_gate)).astype(bf16)

    started += ring_all_gather(tree_b, kv, mixed_all, send_b, recv_b)
    attn_part = jnp.dot(
        mixed_all[...].reshape(rows, DV), vm["w_out"][...], preferred_element_type=f32
    ).astype(bf16)
    width = part_c.shape[2]
    piece = rows // n_tp
    part_c[...] = attn_part.reshape(n_tp, piece, width)
    own_rows = pl.ds(pl.multiple_of(tp * piece, piece), piece)

    started += tp_all_reduce(
        n_tp,
        tp,
        part_c,
        slots_c,
        res_all,
        lambda total: vm["tokens"][own_rows].astype(f32) + total,
        send_c,
        recv_c,
    )
    middle = res_all[...].reshape(rows, width).astype(f32)
    normed_mid = (middle * vm["g_ffn"][...].astype(f32)).astype(bf16)
    units = vm["w_gate"].shape[1]
    padded = part_d.shape[2] // 2
    square_mid = jnp.sum(middle * middle, axis=1, keepdims=True)
    gate_part = jnp.dot(normed_mid, vm["w_gate"][...], preferred_element_type=f32)
    part_d[:, :, :units] = gate_part.astype(bf16).reshape(n_kv, seqs, units)
    rest = padded - units
    part_d[:, :, units:padded] = (
        jnp.broadcast_to(square_mid, (rows, rest)).astype(bf16).reshape(n_kv, seqs, rest)
    )
    up_part = jnp.dot(normed_mid, vm["w_up"][...], preferred_element_type=f32)
    part_d[:, :, padded : padded + units] = up_part.astype(bf16).reshape(n_kv, seqs, units)

    total, sent = ring_reduce_scatter(tree_d, kv, part_d, slots_d, stage_d, send_d, recv_d)
    started += sent
    mid_inverse = lax.rsqrt(total[:, units : units + 1] / D + epsilon)
    gate_sum = total[:, :units] * mid_inverse
    up_sum = total[:, padded : padded + units] * mid_inverse
    hidden_all[kv] = (silu(gate_sum) * up_sum).astype(bf16)

    started += ring_all_gather(tree_e, kv, hidden_all, send_e, recv_e)
    down_part = jnp.dot(
        hidden_all[...].reshape(rows, units), vm["w_down"][...], preferred_element_type=f32
    ).astype(bf16)
    part_f[...] = down_part.reshape(n_tp, piece, width)
    started += tp_all_reduce(
        n_tp,
        tp,
        part_f,
        slots_f,
        out_all,
        lambda total: res_all[tp].astype(f32) + total,
        send_f,
        recv_f,
    )
    out[...] = out_all[...].reshape(rows, width)
    for c in started:
        c.wait_send()


NAMES = (
    "tokens",
    "g_mix",
    "w_query",
    "w_key",
    "w_value",
    "w_outgate",
    "w_decay",
    "cum_decay",
    "step_decay",
    "key_block",
    "value_block",
    "state",
    "g_heads",
    "w_out",
    "g_ffn",
    "w_gate",
    "w_up",
    "w_down",
)


def body(
    tokens,
    lengths,
    state,
    key_block,
    value_block,
    cum_decay,
    step_decay,
    g_mix,
    w_query,
    w_key,
    w_value,
    w_outgate,
    w_decay,
    g_heads,
    w_out,
    g_ffn,
    w_gate,
    w_up,
    w_down,
):
    n_kv = lax.axis_size("kv")
    n_tp = lax.axis_size("tp")
    rows, width = tokens.shape
    seqs = state.shape[0]
    units = w_gate.shape[1]
    piece = rows // n_tp
    arrays = dict(
        tokens=tokens,
        state=state,
        key_block=key_block,
        value_block=value_block,
        cum_decay=cum_decay,
        step_decay=step_decay,
        g_mix=g_mix.reshape(1, -1),
        w_query=w_query,
        w_key=w_key,
        w_value=w_value,
        w_outgate=w_outgate,
        w_decay=w_decay,
        g_heads=g_heads.reshape(1, -1),
        w_out=w_out,
        g_ffn=g_ffn.reshape(1, -1),
        w_gate=w_gate,
        w_up=w_up,
        w_down=w_down,
    )
    trees = tuple(RingTree(n_kv, h) for h in (HUBS_PROJ, HUBS_MIXED, HUBS_FFN, HUBS_HIDDEN))
    wide_a = 3 * DK + 2 * DV + LANES
    wide_d = 2 * (-(-(units + 1) // LANES) * LANES)
    dma = pltpu.SemaphoreType.DMA
    ring_sems = [dma((n_kv - 1,)), dma((n_kv - 1,))]
    tp_sems = [dma((2, n_tp)), dma((2, n_tp))]

    def stage_count(tree):
        return max(2 * (tree.levels() - 1), 1)

    scratch = [pltpu.VMEM(arrays[n].shape, arrays[n].dtype) for n in NAMES]
    scratch += [
        dma((len(NAMES),)),
        pltpu.VMEM((n_kv, seqs, wide_a), bf16),
        pltpu.VMEM((n_kv - 1, seqs, wide_a), bf16),
        pltpu.VMEM((stage_count(trees[0]), seqs, wide_a), bf16),
        pltpu.VMEM((n_kv, seqs, DV), bf16),
        pltpu.VMEM((n_tp, piece, width), bf16),
        pltpu.VMEM((n_tp, piece, width), bf16),
        pltpu.VMEM((n_tp, piece, width), bf16),
        pltpu.VMEM((n_kv, seqs, wide_d), bf16),
        pltpu.VMEM((n_kv - 1, seqs, wide_d), bf16),
        pltpu.VMEM((stage_count(trees[2]), seqs, wide_d), bf16),
        pltpu.VMEM((n_kv, seqs, units), bf16),
        pltpu.VMEM((n_tp, piece, width), bf16),
        pltpu.VMEM((n_tp, piece, width), bf16),
        pltpu.VMEM((n_tp, piece, width), bf16),
    ]
    scratch += ring_sems + ring_sems + tp_sems + ring_sems + ring_sems + tp_sems
    return pl.pallas_call(
        functools.partial(kernel, n_kv, n_tp, trees, NAMES),
        out_shape=jax.ShapeDtypeStruct((rows, width), bf16),
        in_specs=[pl.BlockSpec(memory_space=pltpu.MemorySpace.HBM)] * len(NAMES)
        + [pl.BlockSpec(memory_space=pltpu.MemorySpace.SMEM)],
        out_specs=pl.BlockSpec(memory_space=pltpu.MemorySpace.VMEM),
        scratch_shapes=scratch,
        compiler_params=pltpu.CompilerParams(
            collective_id=0, has_side_effects=True, vmem_limit_bytes=60 << 20
        ),
    )(*[arrays[n] for n in NAMES], lengths)


def solution(mesh):
    return jax.shard_map(
        body,
        mesh=mesh,
        in_specs=(
            P("grp", "kv"),
            P(("grp", "kv")),
            P(("grp", "kv"), "tp", None, None),
            P(("grp", "kv"), "tp", None, None),
            P(("grp", "kv"), "tp", None, None),
            P(("grp", "kv"), "tp", None, None),
            P(("grp", "kv"), "tp"),
            P("kv"),
            P("kv", "tp"),
            P("kv", "tp"),
            P("kv", "tp"),
            P("kv", "tp"),
            P("kv", "tp"),
            P("tp"),
            P("tp", "kv"),
            P("kv"),
            P("kv", "tp"),
            P("kv", "tp"),
            P("tp", "kv"),
        ),
        out_specs=P("grp", "kv"),
        check_vma=False,
    )
```

time: 205 us -> 110 us (0.54)
  blocking collectives: 109 us -> 0 us
  Pallas kernels: 0 us -> 103 us
  starting transfers between devices: 42 us -> 0 us
  waiting for transfers between devices: 31.8 us -> 0 us
  matrix products: 8.44 us -> 0 us
  other arithmetic: 4.23 us -> 0 us
    all_to_all x4 -> x0, blocking collectives: 109 us -> none  [the longest x3 70.8 us: sent_to_all(): return lax.all_to_all(copies, axis, split_axis=0, concat_axis=0, tiled=True)]
    pallas_call x0 -> x1, Pallas kernels: none -> 103 us  [body(): pl.pallas_call(functools.partial(kernel, n_kv, n_tp, trees, NAMES), out_s...]
    all_to_all x3 -> x0, starting transfers between devices: 42 us -> none  [the longest x2 32.8 us: sent_to_all(): return lax.all_to_all(copies, axis, split_axis=0, concat_axis=0, tiled=True)]
    all_to_all x3 -> x0, waiting for transfers between devices: 31.8 us -> none  [the longest x1 20.3 us: summed_on_arrival(): lax.all_to_all(pieces, axis, split_axis=0, concat_axis=0, tiled=True)]
    dot_general x11 -> x0, matrix products: 8.44 us -> none  [the longest x5 5.05 us: body(): jnp.dot(scaled, matrix, preferred_element_type=jnp.float32)]
    unnamed x28 -> x3, local copies, waits for them, and re-layouts: 2.66 us -> 4.94 us
    reduce_sum x10 -> x0, other arithmetic: 2.19 us -> none  [the longest x1 1.1 us: body(): square = jnp.sum(inputs * inputs, axis=1)]
  transfers between devices with their start and end apart: 3 -> 0, of which waited for: 3 -> 0; matrix products, arithmetic and copies ran while one was open for 5% -> 0% of each run, Pallas kernels for 0% -> 0%
where the time goes in v1:
time: 110 us
  Pallas kernels  103 us (94%)
  local copies, waits for them, and re-layouts  6.16 us (6%)
    pallas_call x1, Pallas kernels, body(): pl.pallas_call(functools.partial(kernel, n_kv, n_tp, trees, NAMES), out_s...  103 us
    unnamed x3, local copies, waits for them, and re-layouts  4.94 us

profile of v1, /device:TPU:33, one launch (start us, length us, event | category | flops | bytes accessed | tf_op | source)
XLA Modules:
  0.0 109.6 jit_solution(10287018678489688432)
XLA Ops:
  0.0 1.2 %reshape.10.refs_12_ = bf16[1,256]{1,0:T(2,128)(2,1)} reshape(bf16[256]{0:T(256)(128)(2,1)} %param.32) | data formatting | bytes 1024 | tf_op jit(solution)/shard_map/reshape | solution.py:462
  1.2 1.7 %copy.20.refs_15_ = bf16[128,704]{1,0:T(8,128)(2,1)} copy(bf16[128,704]{0,1:T(8,128)(2,1)} %param.35) | data formatting | bytes 360448 | tf_op args[16]
  2.9 1.7 %copy.21.refs_16_ = bf16[128,704]{1,0:T(8,128)(2,1)} copy(bf16[128,704]{0,1:T(8,128)(2,1)} %param.36) | data formatting | bytes 360448 | tf_op args[17]
  4.7 103.4 %shard_map.181 = bf16[256,128]{1,0:T(8,128)(2,1)} custom-call(bf16[256,128]{1,0:T(8,128)(2,1)} %refs_0_.1, bf16[1,128]{1,0:T(2,128)(2,1)} %bitcast.2, bf16[128,128]{1,0:T(8,128)(2,1)} %refs_2_.1, bf16[128,128]{1,0:T(8,128)(2,1)} %refs_3_.1, bf16[128,256]{1,0:T(8,128)(2,1)} %refs_4_.1, bf16[128,256]{1,0:T(8,128)(2,1)} %refs_5_.1, bf16[128,128]{1,0:T(8,128)(2,1)} %refs_6_.1, ...), custom_call_target="tpu_custom_call" | custom-call | tf_op jit(solution)/shard_map/pallas_call | solution.py:498
  108.1 1.5 %copy.23 = bf16[256,128]{1,0:T(8,128)(2,1)} copy(bf16[256,128]{1,0:T(8,128)(2,1)} %shard_map.181) | data formatting | bytes 131072
